TPU v7x, 32 devices: a whole 2x2x4 slice. The times are simulated.
32 devices in a mesh: sp: 16 (over z, y, core), tp: 2 (over x).
Axes of the slice: x: 2, y: 2, z: 4, core: 2. Of those that a mesh axis runs over, the one named last changes fastest.
Arguments:
- queries: bfloat16 [3072, 1024], P('sp', 'tp'), may hold values from -6 to 6
- keys: bfloat16 [3072, 512], P('sp', 'tp'), may hold values from -6 to 6
- values: bfloat16 [3072, 512], P('sp', 'tp'), may hold values from -6 to 6
- q_gain: float32 [64], replicated, may hold values from 0.1 to 6.5
- k_gain: float32 [64], replicated, may hold values from 0.1 to 6.5
- w_out: bfloat16 [1024, 2048], P('tp'), may hold values from -12 to 12
- residual: bfloat16 [3072, 2048], P(('sp', 'tp')), may hold values from -6 to 6
- norm_gain: float32 [2048], replicated, may hold values from 0.1 to 1.9
- w_gate: bfloat16 [2048, 5632], P('sp', 'tp'), may hold values from -0.125 to 0.125
- w_up: bfloat16 [2048, 5632], P('sp', 'tp'), may hold values from -0.125 to 0.125
- w_down: bfloat16 [5632, 2048], P('tp', 'sp'), may hold values from -0.25 to 0.25
Outputs:
- layer_out: bfloat16 [3072, 2048], P(('sp', 'tp'))
All inputs are finite; a program needn't handle non-finite values.
Results may differ from a plain program's by a relative error of at most 0.018.
The roundings to bfloat16 on the way count: a program that leaves them out, or rounds other values in their place, can miss the bound.
Values may be sent and summed in bfloat16 or wider, within the bound.
A program may use at most 128 MiB of HBM per device.

v0:
```python
import math
import jax
import jax.numpy as jnp
from jax import lax
from jax.sharding import PartitionSpec as P

GRID_W = 128
EPS = 1e-06
THETA = 10000.0


def turn_half(part, angle):
    quarter = part.shape[-1] // 2
    cos_table = jnp.cos(angle)[:, None, :]
    sin_table = jnp.sin(angle)[:, None, :]
    first_part = part[..., :quarter]
    second_part = part[..., quarter:]
    return jnp.concatenate(
        [
            first_part * cos_table - second_part * sin_table,
            first_part * sin_table + second_part * cos_table,
        ],
        axis=-1,
    )


def head_norm_rope(flat, gain, offset, head_count):
    tok_rows = flat.shape[0]
    head_size = flat.shape[1] // head_count
    heads = flat.astype(jnp.float32).reshape(tok_rows, head_count, head_size)
    heads = heads * lax.rsqrt(jnp.mean(heads * heads, axis=-1, keepdims=True) + EPS) * gain
    positions = offset + jnp.arange(tok_rows, dtype=jnp.int32)
    row_pos = (positions // GRID_W).astype(jnp.float32)
    col_pos = (positions % GRID_W).astype(jnp.float32)
    half_size = head_size // 2
    inv_freq = THETA ** (-jnp.arange(0, half_size, 2, dtype=jnp.float32) / half_size)
    turned = jnp.concatenate(
        [
            turn_half(heads[..., :half_size], row_pos[:, None] * inv_freq[None, :]),
            turn_half(heads[..., half_size:], col_pos[:, None] * inv_freq[None, :]),
        ],
        axis=-1,
    )
    return turned.reshape(tok_rows, head_count * head_size).astype(jnp.bfloat16)


def body(queries, keys, values, q_gain, k_gain, w_out, residual, norm_gain, w_gate, w_up, w_down):
    tok_rows = queries.shape[0]
    head_size = q_gain.shape[0]
    q_heads = queries.shape[1] // head_size
    kv_heads = keys.shape[1] // head_size
    q_group = q_heads // kv_heads
    offset = lax.axis_index("sp") * tok_rows
    q_rot = head_norm_rope(queries, q_gain, offset, q_heads)
    k_rot = head_norm_rope(keys, k_gain, offset, kv_heads)
    query_groups = q_rot.reshape(tok_rows, kv_heads, q_group, head_size)
    score_scale = head_size ** (-0.5)
    start_state = (
        jnp.full((kv_heads, q_group, tok_rows), -1e30, jnp.float32),
        jnp.zeros((kv_heads, q_group, tok_rows), jnp.float32),
        jnp.zeros((kv_heads, q_group, tok_rows, head_size), jnp.float32),
    )
    running = start_state
    key_piece = lax.all_gather(k_rot, "sp", axis=0, tiled=True)
    value_piece = lax.all_gather(values, "sp", axis=0, tiled=True)
    piece_len = key_piece.shape[0]
    block_len = math.gcd(piece_len, 512)
    blocks = piece_len // block_len
    key_blocks = key_piece.reshape(blocks, block_len, kv_heads, head_size)
    value_blocks = value_piece.reshape(blocks, block_len, kv_heads, head_size)

    def update(state, block_pair):
        prior_max, totals, accum = state
        key_block, value_block = block_pair
        scores = (
            jnp.einsum(
                "qhgd,khd->hgqk", query_groups, key_block, preferred_element_type=jnp.float32
            )
            * score_scale
        )
        new_max = jnp.maximum(prior_max, jnp.max(scores, axis=-1))
        weights = jnp.exp(scores - new_max[..., None])
        factor = jnp.exp(prior_max - new_max)
        totals = totals * factor + jnp.sum(weights, axis=-1)
        accum = accum * factor[..., None] + jnp.einsum(
            "hgqk,khd->hgqd",
            weights.astype(jnp.bfloat16),
            value_block,
            preferred_element_type=jnp.float32,
        )
        return ((new_max, totals, accum), None)

    running, unused = lax.scan(update, running, (key_blocks, value_blocks))
    final_max, totals, accum = running
    mixed = accum / totals[..., None]
    attn = (
        jnp.transpose(mixed, (2, 0, 1, 3))
        .reshape(tok_rows, q_heads * head_size)
        .astype(jnp.bfloat16)
    )
    own_rows = lax.all_to_all(attn, "tp", split_axis=0, concat_axis=1, tiled=True)
    columns = own_rows
    proj = jnp.dot(
        columns, lax.all_gather(w_out, "tp", axis=0, tiled=True), preferred_element_type=jnp.float32
    )
    mid = residual.astype(jnp.float32) + proj
    normed = (
        mid * lax.rsqrt(jnp.mean(mid * mid, axis=-1, keepdims=True) + EPS) * norm_gain
    ).astype(jnp.bfloat16)
    gathered = lax.all_gather(normed, "tp", axis=0, tiled=True)
    columns = gathered
    gate = jnp.dot(
        columns,
        lax.all_gather(w_gate, "sp", axis=0, tiled=True),
        preferred_element_type=jnp.float32,
    )
    up_part = jnp.dot(
        columns, lax.all_gather(w_up, "sp", axis=0, tiled=True), preferred_element_type=jnp.float32
    )
    hidden = (jax.nn.silu(gate) * up_part).astype(jnp.bfloat16)
    terms = jnp.dot(
        hidden, lax.all_gather(w_down, "sp", axis=1, tiled=True), preferred_element_type=jnp.float32
    )
    down = lax.psum_scatter(
        terms.astype(jnp.bfloat16), "tp", scatter_dimension=0, tiled=True
    ).astype(jnp.float32)
    return (mid + 0.5 * down).astype(jnp.bfloat16)


def solution(mesh):
    return jax.shard_map(
        body,
        mesh=mesh,
        in_specs=(
            P("sp", "tp"),
            P("sp", "tp"),
            P("sp", "tp"),
            P(),
            P(),
            P("tp", None),
            P(("sp", "tp"), None),
            P(),
            P("sp", "tp"),
            P("sp", "tp"),
            P("tp", "sp"),
        ),
        out_specs=P(("sp", "tp"), None),
        check_vma=False,
    )
```

profile of v0, /device:TPU:0, one launch (start us, length us, event | category | flops | bytes accessed | tf_op | source)
XLA Modules:
  0.0 477.9 jit_solution(934830852998414411)
XLA Ops:
  6.6 1.0 copy.23
  7.7 0.7 fusion.24
  8.4 0.2 multiply_cosine_fusion.1
  8.7 0.7 copy.24
  9.5 0.7 all-gather.9.cloned.1.call-update
  10.3 0.7 all-gather.11.cloned.1.call-update
  11.0 0.5 all-gather.13.cloned.1.call-update
  11.6 0.5 all-gather.15.cloned.1.call-update
  12.2 0.5 all-gather.17.cloned.1.call-update
  12.8 0.1 copy.26
  12.9 0.1 fusion.21
  13.1 0.1 fusion.22
  13.2 0.1 subtract_convert_fusion.1
  13.3 38.7 %all-gather.7.cloned.1.call-done = bf16[3072,256]{1,0:T(8,128)(2,1)} async-done(((bf16[192,256]{1,0:T(8,128)(2,1)}), bf16[3072,256]{1,0:T(8,128)(2,1)}) %all-gather.7.cloned.1.call-update) | async-done | bytes 1572880 | tf_op jit(solution)/shard_map/all_gather | solution.py:64
  52.0 4.6 reshape.207
  56.6 3.3 copy.28
  59.9 32.7 %all-gather.9.cloned.1.call-done = bf16[3072,256]{1,0:T(8,128)(2,1)} async-done(((bf16[192,256]{1,0:T(8,128)(2,1)}), bf16[3072,256]{1,0:T(8,128)(2,1)}) %all-gather.9.cloned.1.call-update) | async-done | bytes 1572880 | tf_op jit(solution)/shard_map/all_gather | solution.py:65
  92.6 4.6 reshape.208
  97.2 3.3 copy.29
  100.5 32.2 %while.15 = (s32[]{:T(128)}, f32[4,2,192]{2,1,0:T(2,128)S(1)}, f32[4,2,192]{2,1,0:T(2,128)S(1)}, f32[4,2,192,64]{2,3,1,0:T(8,128)}, bf16[6,512,4,64]{1,3,2,0:T(8...) while((s32[]{:T(128)}, f32[4,2,192]{2,1,0:T(2,128)S(1)}, ...), condition=%wide.region_5.6_spmd.clone, body=%wide.region_2.5_spmd.clone.sunk | while | flops 207920640 | bytes 14189729 | solution.py:93
  100.5 1.7 bitcast_reduce_fusion.2
  102.3 0.9 fusion.50
  103.2 0.1 copy-done
  103.4 1.8 fusion.52
  105.2 0.8 copy-done.1
  106.0 1.7 bitcast_reduce_fusion.2
  107.7 0.9 fusion.50
  108.7 0.1 copy-done
  108.7 1.8 fusion.52
  110.5 0.8 copy-done.1
  111.4 1.7 bitcast_reduce_fusion.2
  113.1 0.9 fusion.50
  114.1 1.8 fusion.52
  115.9 0.8 copy-done.1
  116.7 1.7 bitcast_reduce_fusion.2
  118.4 0.9 fusion.50
  119.4 0.1 copy-done
  119.4 1.8 fusion.52
  121.3 0.8 copy-done.1
  122.1 1.7 bitcast_reduce_fusion.2
  123.8 0.9 fusion.50
  124.7 0.1 copy-done
  124.8 1.8 fusion.52
  126.6 0.8 copy-done.1
  127.4 1.7 bitcast_reduce_fusion.2
  129.1 0.9 fusion.50
  130.1 0.1 copy-done
  130.2 1.8 fusion.52
  132.0 0.8 copy-done.1
  132.8 1.1 fusion.25
  133.9 0.2 convert_element_type.65
  134.0 0.2 copy.30
  134.2 10.3 %all_to_all.16 = bf16[2,96,512]{2,1,0:T(8,128)(2,1)S(1)} all-to-all(bf16[2,96,512]{2,1,0:T(8,128)(2,1)S(1)} %copy.30), channel_id=1, replica_groups=mesh['sp'=16,'tp'=2] {'tp'}, dimensions={0} | all-to-all | bytes 393216 | tf_op jit(solution)/shard_map/all_to_all | solution.py:101
  144.5 7.2 %all-gather.11.cloned.1.call-done = bf16[1024,2048]{1,0:T(8,128)(2,1)} async-done(((bf16[512,2048]{1,0:T(8,128)(2,1)}), bf16[1024,2048]{1,0:T(8,128)(2,1)}) %all-gather.11.cloned.1.call-update) | async-done | bytes 4194320 | tf_op jit(solution)/shard_map/all_gather | solution.py:104
  151.7 3.2 multiply_reduce_fusion
  154.9 0.1 multiply_convert_fusion
  155.1 11.5 %all_gather.24 = bf16[192,2048]{1,0:T(8,128)(2,1)S(1)} all-gather(bf16[96,2048]{1,0:T(8,128)(2,1)S(1)} %multiply_convert_fusion), channel_id=1, replica_groups=mesh['sp'=16,'tp'=2] {'tp'}, dimensions={0}, use_global_device_ids=true | all-gather | bytes 1179648 | tf_op jit(solution)/shard_map/all_gather | solution.py:110
  166.6 81.3 %all-gather.13.cloned.1.call-done = bf16[2048,2816]{1,0:T(8,128)(2,1)} async-done(((bf16[128,2816]{1,0:T(8,128)(2,1)}), bf16[2048,2816]{1,0:T(8,128)(2,1)}) %all-gather.13.cloned.1.call-update) | async-done | bytes 11534352 | tf_op jit(solution)/shard_map/all_gather | solution.py:114
  247.9 8.0 %fusion.30 = f32[192,2816]{1,0:T(8,128)} fusion(bf16[192,2048]{1,0:T(8,128)(2,1)S(1)} %all_gather.24, bf16[2048,2816]{1,0:T(8,128)(2,1)} %all-gather.13.cloned.1.call-done), kind=kOutput, calls=%fused_computation.69 | convolution fusion | flops 2214592512 | bytes 14483456 | tf_op jit(solution)/shard_map/dot_general | solution.py:112
  255.9 86.4 %all-gather.15.cloned.1.call-done = bf16[2048,2816]{1,0:T(8,128)(2,1)} async-done(((bf16[128,2816]{1,0:T(8,128)(2,1)}), bf16[2048,2816]{1,0:T(8,128)(2,1)}) %all-gather.15.cloned.1.call-update) | async-done | bytes 11534352 | tf_op jit(solution)/shard_map/all_gather | solution.py:118
  342.3 97.2 %all-gather.17.cloned.1.call-done = bf16[2816,2048]{1,0:T(8,128)(2,1)} async-done(((bf16[2816,128]{1,0:T(8,128)(2,1)}), bf16[2816,2048]{1,0:T(8,128)(2,1)}) %all-gather.17.cloned.1.call-update) | async-done | bytes 11534352 | tf_op jit(solution)/shard_map/all_gather | solution.py:122
  439.4 13.9 %convolution_convert_fusion = bf16[192,2048]{1,0:T(8,128)(2,1)} fusion(bf16[2816,2048]{1,0:T(8,128)(2,1)} %all-gather.17.cloned.1.call-done, bf16[192,2048]{1,0:T(8,128)(2,1)S(1)} %all_gather.24, bf16[2048,2816]{1,0:T(8,128)(2,1)} %all-gather.15.cloned.1.call-done, f32[192,2816]{1,0:T(8,128)} %fusion.30), kind=kOutput, calls=%fused_computation.25 | convolution fusion | flops 4432822272 | bytes 26804224 | tf_op jit(solution)/shard_map/dot_general | solution.py:121
  453.3 15.8 %reduce-scatter.2.cloned.1.call-done = bf16[96,2048]{1,0:T(8,128)(2,1)} async-done(((bf16[192,2048]{1,0:T(8,128)(2,1)}), bf16[96,2048]{1,0:T(8,128)(2,1)}) %reduce-scatter.2.cloned.1.call-update) | async-done | bytes 393232 | tf_op jit(solution)/shard_map/reduce_scatter | solution.py:124
  469.2 1.8 add_convert_fusion
  (59 shorter events, 0.8 us)
Async XLA Ops:
  6.5 6.3 %copy-start.2 = (bf16[192,512]{1,0:T(8,128)(2,1)S(1)}, bf16[192,512]{1,0:T(8,128)(2,1)}, u32[]{:S(2)}) copy-start(bf16[192,512]{1,0:T(8,128)(2,1)} %param.13) | copy-start | bytes 589828
  6.5 45.4 %all-gather.7.cloned.1.call-start = ((), (), s32[]{:S(2)}) async-start(), calls=%async_computation.2 | async-start | bytes 1671168 | tf_op jit(solution)/shard_map/all_gather | solution.py:64
  8.4 4.6 copy-start.4
  9.5 83.1 %all-gather.9.cloned.1.call-start = ((), (), s32[]{:S(2)}) async-start(), calls=%async_computation.3 | async-start | bytes 1671168 | tf_op jit(solution)/shard_map/all_gather | solution.py:65
  10.2 141.5 %all-gather.11.cloned.1.call-start = ((), (), s32[]{:S(2)}) async-start(), calls=%async_computation.4 | async-start | bytes 6291456 | tf_op jit(solution)/shard_map/all_gather | solution.py:104
  11.0 236.9 %all-gather.13.cloned.1.call-start = ((), (), s32[]{:S(2)}) async-start(), calls=%async_computation.5 | async-start | bytes 12255232 | tf_op jit(solution)/shard_map/all_gather | solution.py:114
  11.6 330.7 %all-gather.15.cloned.1.call-start = ((), (), s32[]{:S(2)}) async-start(), calls=%async_computation.6 | async-start | bytes 12255232 | tf_op jit(solution)/shard_map/all_gather | solution.py:118
  12.1 427.3 %all-gather.17.cloned.1.call-start = ((), (), s32[]{:S(2)}) async-start(), calls=%async_computation.7 | async-start | bytes 12255232 | tf_op jit(solution)/shard_map/all_gather | solution.py:122
  12.7 456.4 %reduce-scatter.2.cloned.1.call-start = ((), (), s32[]{:S(2)}) async-start(), calls=%async_computation.8 | async-start | bytes 1179648 | tf_op jit(solution)/shard_map/reduce_scatter | solution.py:124
  102.3 1.1 copy-start
  105.2 0.8 copy-start.1
  107.7 1.0 copy-start
  110.5 0.8 copy-start.1
  113.0 1.0 copy-start
  115.9 0.8 copy-start.1
  118.4 1.0 copy-start
  121.2 0.8 copy-start.1
  123.8 1.0 copy-start
  126.6 0.8 copy-start.1
  129.1 1.0 copy-start
  132.0 0.8 copy-start.1
  134.2 20.7 %copy-start.3 = (f32[2048]{0:T(1024)S(1)}, f32[2048]{0:T(1024)}, u32[]{:S(2)}) copy-start(f32[2048]{0:T(1024)} %param.20) | copy-start | bytes 24580
Sparse Core Ops, SparseCore 0:
  9.6 42.3 all-gather.6
  54.3 38.2 all-gather.8
  94.1 57.5 all-gather.10
  153.9 93.9 all-gather.12
  250.0 92.2 all-gather.14
  344.3 95.1 all-gather.16
  453.4 15.6 reduce-scatter.1
where the time goes:
time: 479 us; the launch traced here: 478 us
  waiting for transfers between devices  362 us (76%)
  matrix products  46 us (10%)
  local copies, waits for them, and re-layouts  23.4 us (5%)
  blocking collectives  21.8 us (5%)
  between operations  13.7 us (3%)
  other arithmetic  10.2 us (2%)
    all_gather x1, waiting for transfers between devices, body(): lax.all_gather(w_down, 'sp', axis=1, tiled=True)  97.2 us
    all_gather x1, waiting for transfers between devices, body(): lax.all_gather(w_up, 'sp', axis=0, tiled=True)  86.4 us
    all_gather x1, waiting for transfers between devices, body(): lax.all_gather(w_gate, 'sp', axis=0, tiled=True)  81.3 us
    all_gather x1, waiting for transfers between devices, body(): key_piece = lax.all_gather(k_rot, 'sp', axis=0, tiled=True)  38.7 us
    all_gather x1, waiting for transfers between devices, body(): value_piece = lax.all_gather(values, 'sp', axis=0, tiled=True)  32.7 us
    reduce_scatter x1, waiting for transfers between devices, body(): lax.psum_scatter(terms.astype(jnp.bfloat16), 'tp', scatter_dimension=0, t...  15.8 us
    dot_general x1, matrix products, body(): jnp.dot(hidden, lax.all_gather(w_down, 'sp', axis=1, tiled=True), preferr...  13.9 us
    all_gather x1, blocking collectives, body(): gathered = lax.all_gather(normed, 'tp', axis=0, tiled=True)  11.5 us
  transfers between devices with their start and end apart: 7, of which 7 were waited for; matrix products, arithmetic and copies ran while one was open for 12% of the time, Pallas kernels for 0%

commit v1 on v0

--- a/solution.py
+++ b/solution.py
@@ -1,3 +1,4 @@
+import functools
 import math
 import jax
 import jax.numpy as jnp
@@ -7,6 +8,25 @@
 GRID_W = 128
 EPS = 1e-06
 THETA = 10000.0
+
+
+def serve_strips_all_in(mine, shard_axis, along_dim):
+    slots = lax.axis_size(shard_axis)
+    cards = tuple(((src_i, (src_i + 1) % slots) for src_i in range(slots)))
+
+    def begin_types_for(carry_out):
+        if len(carry_out) == slots:
+            return carry_out
+        return begin_types_for([lax.ppermute(carry_out[0], shard_axis, cards), *carry_out])
+
+    return jnp.roll(
+        jnp.concatenate(begin_types_for([mine]), along_dim),
+        (lax.axis_index(shard_axis) + 1) * mine.shape[along_dim],
+        along_dim,
+    )
+
+
+take_the_classes = functools.partial(serve_strips_all_in, shard_axis="sp", along_dim=0)
 
 
 def turn_half(part, angle):
@@ -62,7 +82,7 @@
     )
     running = start_state
     key_piece = lax.all_gather(k_rot, "sp", axis=0, tiled=True)
-    value_piece = lax.all_gather(values, "sp", axis=0, tiled=True)
+    value_piece = take_the_classes(values)
     piece_len = key_piece.shape[0]
     block_len = math.gcd(piece_len, 512)
     blocks = piece_len // block_len

time: 479 us -> 438 us (0.914)
  waiting for transfers between devices: 362 us -> 324 us
  blocking collectives: 21.8 us -> 16.2 us
    ppermute x0 -> x15, waiting for transfers between devices: none -> 103 us  [begin_types_for(): lax.ppermute(carry_out[0], shard_axis, cards)]
    all_gather x1, waiting for transfers between devices: 81.3 us -> 18.9 us  [body(): lax.all_gather(w_gate, 'sp', axis=0, tiled=True)]
    all_gather x1, waiting for transfers between devices: 38.7 us -> 0.01 us  [body(): key_piece = lax.all_gather(k_rot, 'sp', axis=0, tiled=True)]
    all_gather x1 -> x0, waiting for transfers between devices: 32.7 us -> none  [body(): value_piece = lax.all_gather(values, 'sp', axis=0, tiled=True)]
    all_gather x1, waiting for transfers between devices: 7.22 us -> 0.02 us  [body(): lax.all_gather(w_out, 'tp', axis=0, tiled=True)]
  transfers between devices with their start and end apart: 7 -> 21, of which waited for: 7 -> 19; matrix products, arithmetic and copies ran while one was open for 12% -> 13% of each run, Pallas kernels for 0% -> 0%
where the time goes in v1:
time: 438 us; the launch traced here: 437 us
  waiting for transfers between devices  324 us (74%)
  matrix products  45.9 us (10%)
  local copies, waits for them, and re-layouts  25.3 us (6%)
  blocking collectives  16.2 us (4%)
  between operations  14 us (3%)
  other arithmetic  10.2 us (2%)
    ppermute x15, waiting for transfers between devices, begin_types_for(): lax.ppermute(carry_out[0], shard_axis, cards)  103 us
    all_gather x1, waiting for transfers between devices, body(): lax.all_gather(w_down, 'sp', axis=1, tiled=True)  97.2 us
    all_gather x1, waiting for transfers between devices, body(): lax.all_gather(w_up, 'sp', axis=0, tiled=True)  86.4 us
    all_gather x1, waiting for transfers between devices, body(): lax.all_gather(w_gate, 'sp', axis=0, tiled=True)  18.9 us
    reduce_scatter x1, waiting for transfers between devices, body(): lax.psum_scatter(terms.astype(jnp.bfloat16), 'tp', scatter_dimension=0, t...  15.8 us
    dot_general x1, matrix products, body(): jnp.dot(hidden, lax.all_gather(w_down, 'sp', axis=1, tiled=True), preferr...  13.8 us
    dot_general x6, matrix products, update(): jnp.einsum('hgqk,khd->hgqd', weights.astype(jnp.bfloat16), value_block, p...  10.9 us
    dot_general x6, matrix products, update(): jnp.einsum('qhgd,khd->hgqk', query_groups, key_block, preferred_element_t...  10.1 us
  transfers between devices with their start and end apart: 21, of which 19 were waited for; matrix products, arithmetic and copies ran while one was open for 13% of the time, Pallas kernels for 0%

profile of v1, /device:TPU:0, one launch (start us, length us, event | category | flops | bytes accessed | tf_op | source)
XLA Modules:
  0.0 436.6 jit_solution(17746204949857592274)
XLA Ops:
  6.6 1.1 copy.23
  7.7 0.7 fusion.24
  8.7 0.7 copy.24
  9.6 0.7 all-gather.8.cloned.1.call-update
  10.3 0.7 all-gather.10.cloned.1.call-update
  11.0 0.5 all-gather.12.cloned.1.call-update
  11.6 0.5 all-gather.14.cloned.1.call-update
  12.2 0.5 collective-permute-start
  12.8 7.3 %collective-permute-done = bf16[192,256]{1,0:T(8,128)(2,1)S(1)} collective-permute-done((bf16[192,256]{1,0:T(8,128)(2,1)S(1)}, bf16[192,256]{1,0:T(8,128)(2,1)S(1)}, u32[]{:S(2)}, u32[]{:S(2)}) %collective-permute-start) | collective-permute-done | bytes 98336 | tf_op jit(solution)/shard_map/ppermute | solution.py:20
  20.0 7.8 %collective-permute-done.1 = bf16[192,256]{1,0:T(8,128)(2,1)S(1)} collective-permute-done((bf16[192,256]{1,0:T(8,128)(2,1)S(1)}, bf16[192,256]{1,0:T(8,128)(2,1)S(1)}, u32[]{:S(2)}, u32[]{:S(2)}) %collective-permute-start.1) | collective-permute-done | bytes 98336 | tf_op jit(solution)/shard_map/ppermute | solution.py:20
  27.9 6.9 %collective-permute-done.2 = bf16[192,256]{1,0:T(8,128)(2,1)S(1)} collective-permute-done((bf16[192,256]{1,0:T(8,128)(2,1)S(1)}, bf16[192,256]{1,0:T(8,128)(2,1)S(1)}, u32[]{:S(2)}, u32[]{:S(2)}) %collective-permute-start.2) | collective-permute-done | bytes 98336 | tf_op jit(solution)/shard_map/ppermute | solution.py:20
  34.8 6.9 %collective-permute-done.3 = bf16[192,256]{1,0:T(8,128)(2,1)S(1)} collective-permute-done((bf16[192,256]{1,0:T(8,128)(2,1)S(1)}, bf16[192,256]{1,0:T(8,128)(2,1)S(1)}, u32[]{:S(2)}, u32[]{:S(2)}) %collective-permute-start.3) | collective-permute-done | bytes 98336 | tf_op jit(solution)/shard_map/ppermute | solution.py:20
  41.7 7.4 %collective-permute-done.4 = bf16[192,256]{1,0:T(8,128)(2,1)S(1)} collective-permute-done((bf16[192,256]{1,0:T(8,128)(2,1)S(1)}, bf16[192,256]{1,0:T(8,128)(2,1)S(1)}, u32[]{:S(2)}, u32[]{:S(2)}) %collective-permute-start.4) | collective-permute-done | bytes 98336 | tf_op jit(solution)/shard_map/ppermute | solution.py:20
  49.1 6.7 %collective-permute-done.5 = bf16[192,256]{1,0:T(8,128)(2,1)S(1)} collective-permute-done((bf16[192,256]{1,0:T(8,128)(2,1)S(1)}, bf16[192,256]{1,0:T(8,128)(2,1)S(1)}, u32[]{:S(2)}, u32[]{:S(2)}) %collective-permute-start.5) | collective-permute-done | bytes 98336 | tf_op jit(solution)/shard_map/ppermute | solution.py:20
  55.8 6.7 %collective-permute-done.6 = bf16[192,256]{1,0:T(8,128)(2,1)S(1)} collective-permute-done((bf16[192,256]{1,0:T(8,128)(2,1)S(1)}, bf16[192,256]{1,0:T(8,128)(2,1)S(1)}, u32[]{:S(2)}, u32[]{:S(2)}) %collective-permute-start.6) | collective-permute-done | bytes 98336 | tf_op jit(solution)/shard_map/ppermute | solution.py:20
  62.6 6.7 %collective-permute-done.7 = bf16[192,256]{1,0:T(8,128)(2,1)S(1)} collective-permute-done((bf16[192,256]{1,0:T(8,128)(2,1)S(1)}, bf16[192,256]{1,0:T(8,128)(2,1)S(1)}, u32[]{:S(2)}, u32[]{:S(2)}) %collective-permute-start.7) | collective-permute-done | bytes 98336 | tf_op jit(solution)/shard_map/ppermute | solution.py:20
  69.3 6.7 %collective-permute-done.8 = bf16[192,256]{1,0:T(8,128)(2,1)S(1)} collective-permute-done((bf16[192,256]{1,0:T(8,128)(2,1)S(1)}, bf16[192,256]{1,0:T(8,128)(2,1)S(1)}, u32[]{:S(2)}, u32[]{:S(2)}) %collective-permute-start.8) | collective-permute-done | bytes 98336 | tf_op jit(solution)/shard_map/ppermute | solution.py:20
  76.2 6.6 %collective-permute-done.9 = bf16[192,256]{1,0:T(8,128)(2,1)S(1)} collective-permute-done((bf16[192,256]{1,0:T(8,128)(2,1)S(1)}, bf16[192,256]{1,0:T(8,128)(2,1)S(1)}, u32[]{:S(2)}, u32[]{:S(2)}) %collective-permute-start.9) | collective-permute-done | bytes 98336 | tf_op jit(solution)/shard_map/ppermute | solution.py:20
  82.9 6.7 %collective-permute-done.10 = bf16[192,256]{1,0:T(8,128)(2,1)S(1)} collective-permute-done((bf16[192,256]{1,0:T(8,128)(2,1)S(1)}, bf16[192,256]{1,0:T(8,128)(2,1)S(1)}, u32[]{:S(2)}, u32[]{:S(2)}) %collective-permute-start.10) | collective-permute-done | bytes 98336 | tf_op jit(solution)/shard_map/ppermute | solution.py:20
  89.6 6.7 %collective-permute-done.11 = bf16[192,256]{1,0:T(8,128)(2,1)S(1)} collective-permute-done((bf16[192,256]{1,0:T(8,128)(2,1)S(1)}, bf16[192,256]{1,0:T(8,128)(2,1)S(1)}, u32[]{:S(2)}, u32[]{:S(2)}) %collective-permute-start.11) | collective-permute-done | bytes 98336 | tf_op jit(solution)/shard_map/ppermute | solution.py:20
  96.4 6.6 %collective-permute-done.12 = bf16[192,256]{1,0:T(8,128)(2,1)S(1)} collective-permute-done((bf16[192,256]{1,0:T(8,128)(2,1)S(1)}, bf16[192,256]{1,0:T(8,128)(2,1)S(1)}, u32[]{:S(2)}, u32[]{:S(2)}) %collective-permute-start.12) | collective-permute-done | bytes 98336 | tf_op jit(solution)/shard_map/ppermute | solution.py:20
  103.2 6.6 %collective-permute-done.13 = bf16[192,256]{1,0:T(8,128)(2,1)S(1)} collective-permute-done((bf16[192,256]{1,0:T(8,128)(2,1)S(1)}, bf16[192,256]{1,0:T(8,128)(2,1)S(1)}, u32[]{:S(2)}, u32[]{:S(2)}) %collective-permute-start.13) | collective-permute-done | bytes 98336 | tf_op jit(solution)/shard_map/ppermute | solution.py:20
  109.8 6.7 %collective-permute-done.14 = bf16[192,256]{1,0:T(8,128)(2,1)S(1)} collective-permute-done((bf16[192,256]{1,0:T(8,128)(2,1)S(1)}, bf16[192,256]{1,0:T(8,128)(2,1)S(1)}, u32[]{:S(2)}, u32[]{:S(2)}) %collective-permute-start.14) | collective-permute-done | bytes 98336 | tf_op jit(solution)/shard_map/ppermute | solution.py:20
  117.0 1.6 constant_dynamic-slice_fusion
  118.6 4.6 %reshape.208 = bf16[6,512,4,64]{3,2,1,0:T(4,128)(2,1)S(1)} reshape(bf16[3072,256]{1,0:T(8,128)(2,1)} %constant_dynamic-slice_fusion) | data formatting | bytes 3145728 | tf_op jit(solution)/shard_map/reshape | solution.py:90
  123.2 3.3 copy.29
  126.6 4.6 %reshape.207 = bf16[6,512,4,64]{3,2,1,0:T(4,128)(2,1)S(1)} reshape(bf16[3072,256]{1,0:T(8,128)(2,1)} %all-gather.6.cloned.1.call-done) | data formatting | bytes 3145728 | tf_op jit(solution)/shard_map/reshape | solution.py:89
  131.2 3.3 copy.28
  134.5 32.2 %while.15 = (s32[]{:T(128)}, f32[4,2,192]{2,1,0:T(2,128)S(1)}, f32[4,2,192]{2,1,0:T(2,128)S(1)}, f32[4,2,192,64]{2,3,1,0:T(8,128)}, bf16[6,512,4,64]{1,3,2,0:T(8...) while((s32[]{:T(128)}, f32[4,2,192]{2,1,0:T(2,128)S(1)}, ...), condition=%wide.region_5.6_spmd.clone, body=%wide.region_2.5_spmd.clone.sunk | while | flops 207920640 | bytes 14189729 | solution.py:113
  134.5 1.7 bitcast_reduce_fusion.2
  136.2 0.9 fusion.50
  137.2 1.8 fusion.52
  139.1 0.8 copy-done.1
  139.8 1.7 bitcast_reduce_fusion.2
  141.6 0.9 fusion.50
  142.6 1.8 fusion.52
  144.4 0.8 copy-done.1
  145.2 1.7 bitcast_reduce_fusion.2
  146.9 0.9 fusion.50
  147.9 1.8 fusion.52
  149.7 0.8 copy-done.1
  150.5 1.7 bitcast_reduce_fusion.2
  152.2 0.9 fusion.50
  153.4 1.8 fusion.52
  155.3 0.8 copy-done.1
  156.1 1.7 bitcast_reduce_fusion.2
  157.8 0.9 fusion.50
  158.8 1.8 fusion.52
  160.6 0.8 copy-done.1
  161.4 1.7 bitcast_reduce_fusion.2
  163.1 0.9 fusion.50
  164.1 1.8 fusion.52
  166.0 0.8 copy-done.1
  166.8 1.1 fusion.25
  168.2 7.6 %all_to_all.16 = bf16[2,96,512]{2,1,0:T(8,128)(2,1)S(1)} all-to-all(bf16[2,96,512]{2,1,0:T(8,128)(2,1)S(1)} %copy.30), channel_id=1, replica_groups=mesh['sp'=16,'tp'=2] {'tp'}, dimensions={0} | all-to-all | bytes 393216 | tf_op jit(solution)/shard_map/all_to_all | solution.py:121
  175.8 3.2 multiply_reduce_fusion
  179.2 8.6 %all_gather.20 = bf16[192,2048]{1,0:T(8,128)(2,1)S(1)} all-gather(bf16[96,2048]{1,0:T(8,128)(2,1)S(1)} %multiply_convert_fusion), channel_id=1, replica_groups=mesh['sp'=16,'tp'=2] {'tp'}, dimensions={0}, use_global_device_ids=true | all-gather | bytes 1179648 | tf_op jit(solution)/shard_map/all_gather | solution.py:130
  187.8 18.9 %all-gather.10.cloned.1.call-done = bf16[2048,2816]{1,0:T(8,128)(2,1)} async-done(((bf16[128,2816]{1,0:T(8,128)(2,1)}), bf16[2048,2816]{1,0:T(8,128)(2,1)}) %all-gather.10.cloned.1.call-update) | async-done | bytes 11534352 | tf_op jit(solution)/shard_map/all_gather | solution.py:134
  206.7 8.0 %fusion.30 = f32[192,2816]{1,0:T(8,128)} fusion(bf16[192,2048]{1,0:T(8,128)(2,1)S(1)} %all_gather.20, bf16[2048,2816]{1,0:T(8,128)(2,1)} %all-gather.10.cloned.1.call-done), kind=kOutput, calls=%fused_computation.102 | convolution fusion | flops 2214592512 | bytes 14483456 | tf_op jit(solution)/shard_map/dot_general | solution.py:132
  214.7 86.4 %all-gather.12.cloned.1.call-done = bf16[2048,2816]{1,0:T(8,128)(2,1)} async-done(((bf16[128,2816]{1,0:T(8,128)(2,1)}), bf16[2048,2816]{1,0:T(8,128)(2,1)}) %all-gather.12.cloned.1.call-update) | async-done | bytes 11534352 | tf_op jit(solution)/shard_map/all_gather | solution.py:138
  301.1 97.2 %all-gather.14.cloned.1.call-done = bf16[2816,2048]{1,0:T(8,128)(2,1)} async-done(((bf16[2816,128]{1,0:T(8,128)(2,1)}), bf16[2816,2048]{1,0:T(8,128)(2,1)}) %all-gather.14.cloned.1.call-update) | async-done | bytes 11534352 | tf_op jit(solution)/shard_map/all_gather | solution.py:142
  398.3 13.8 %convolution_convert_fusion = bf16[192,2048]{1,0:T(8,128)(2,1)} fusion(bf16[2816,2048]{1,0:T(8,128)(2,1)} %all-gather.14.cloned.1.call-done, bf16[192,2048]{1,0:T(8,128)(2,1)S(1)} %all_gather.20, bf16[2048,2816]{1,0:T(8,128)(2,1)} %all-gather.12.cloned.1.call-done, f32[192,2816]{1,0:T(8,128)} %fusion.30), kind=kOutput, calls=%fused_computation.25 | convolution fusion | flops 4432822272 | bytes 26804224 | tf_op jit(solution)/shard_map/dot_general | solution.py:141
  412.1 15.8 %reduce-scatter.2.cloned.1.call-done = bf16[96,2048]{1,0:T(8,128)(2,1)} async-done(((bf16[192,2048]{1,0:T(8,128)(2,1)}), bf16[96,2048]{1,0:T(8,128)(2,1)}) %reduce-scatter.2.cloned.1.call-update) | async-done | bytes 393232 | tf_op jit(solution)/shard_map/reduce_scatter | solution.py:144
  427.9 1.8 add_convert_fusion
  (121 shorter events, 2.6 us)
Async XLA Ops:
  6.5 5.7 %copy-start.2 = (bf16[192,256]{1,0:T(8,128)(2,1)S(1)}, bf16[192,256]{1,0:T(8,128)(2,1)}, u32[]{:S(2)}) copy-start(bf16[192,256]{1,0:T(8,128)(2,1)} %param.15) | copy-start | bytes 294916
  6.5 69.5 %copy-start.3 = (bf16[192,512]{1,0:T(8,128)(2,1)S(1)}, bf16[192,512]{1,0:T(8,128)(2,1)}, u32[]{:S(2)}) copy-start(bf16[192,512]{1,0:T(8,128)(2,1)} %param.13) | copy-start | bytes 589828
  6.5 120.0 %all-gather.6.cloned.1.call-start = ((), (), s32[]{:S(2)}) async-start(), calls=%async_computation.2 | async-start | bytes 1671168 | tf_op jit(solution)/shard_map/all_gather | solution.py:84
  8.4 87.8 %copy-start.5 = (f32[64]{0:T(128)S(1)}, f32[64]{0:T(128)}, u32[]{:S(2)}) copy-start(f32[64]{0:T(128)} %param.16) | copy-start | bytes 772
  9.5 166.3 %all-gather.8.cloned.1.call-start = ((), (), s32[]{:S(2)}) async-start(), calls=%async_computation.3 | async-start | bytes 6291456 | tf_op jit(solution)/shard_map/all_gather | solution.py:124
  10.3 196.4 %all-gather.10.cloned.1.call-start = ((), (), s32[]{:S(2)}) async-start(), calls=%async_computation.4 | async-start | bytes 12255232 | tf_op jit(solution)/shard_map/all_gather | solution.py:134
  11.0 290.1 %all-gather.12.cloned.1.call-start = ((), (), s32[]{:S(2)}) async-start(), calls=%async_computation.5 | async-start | bytes 12255232 | tf_op jit(solution)/shard_map/all_gather | solution.py:138
  11.6 386.7 %all-gather.14.cloned.1.call-start = ((), (), s32[]{:S(2)}) async-start(), calls=%async_computation.6 | async-start | bytes 12255232 | tf_op jit(solution)/shard_map/all_gather | solution.py:142
  12.2 415.8 %reduce-scatter.2.cloned.1.call-start = ((), (), s32[]{:S(2)}) async-start(), calls=%async_computation.7 | async-start | bytes 1179648 | tf_op jit(solution)/shard_map/reduce_scatter | solution.py:144
  12.2 7.8 %collective-permute-start = (bf16[192,256]{1,0:T(8,128)(2,1)S(1)}, bf16[192,256]{1,0:T(8,128)(2,1)S(1)}, u32[]{:S(2)}, u32[]{:S(2)}) collective-permute-start(bf16[192,256]{1,0:T(8,128)(2,1)S(1)} %copy-done.2), channel_id=1, source_target_pairs={{0,2},{2,4},{4,6},{6,8},{8,10},{10,12},{12,14},{14,16},{16,18},{18... | collective-permute-start | bytes 294920 | tf_op jit(solution)/shard_map/ppermute | solution.py:20
  20.0 7.8 %collective-permute-start.1 = (bf16[192,256]{1,0:T(8,128)(2,1)S(1)}, bf16[192,256]{1,0:T(8,128)(2,1)S(1)}, u32[]{:S(2)}, u32[]{:S(2)}) collective-permute-start(bf16[192,256]{1,0:T(8,128)(2,1)S(1)} %collective-permute-done), channel_id=1, source_target_pairs={{0,2},{2,4},{4,6},{6,8},{8,10},{10,12},{12,14},{14,16},{16,18},{18... | collective-permute-start | bytes 294920 | tf_op jit(solution)/shard_map/ppermute | solution.py:20
  27.9 6.9 %collective-permute-start.2 = (bf16[192,256]{1,0:T(8,128)(2,1)S(1)}, bf16[192,256]{1,0:T(8,128)(2,1)S(1)}, u32[]{:S(2)}, u32[]{:S(2)}) collective-permute-start(bf16[192,256]{1,0:T(8,128)(2,1)S(1)} %collective-permute-done.1), channel_id=1, source_target_pairs={{0,2},{2,4},{4,6},{6,8},{8,10},{10,12},{12,14},{14,16},{16,18},{18... | collective-permute-start | bytes 294920 | tf_op jit(solution)/shard_map/ppermute | solution.py:20
  34.8 6.9 %collective-permute-start.3 = (bf16[192,256]{1,0:T(8,128)(2,1)S(1)}, bf16[192,256]{1,0:T(8,128)(2,1)S(1)}, u32[]{:S(2)}, u32[]{:S(2)}) collective-permute-start(bf16[192,256]{1,0:T(8,128)(2,1)S(1)} %collective-permute-done.2), channel_id=1, source_target_pairs={{0,2},{2,4},{4,6},{6,8},{8,10},{10,12},{12,14},{14,16},{16,18},{18... | collective-permute-start | bytes 294920 | tf_op jit(solution)/shard_map/ppermute | solution.py:20
  41.7 7.4 %collective-permute-start.4 = (bf16[192,256]{1,0:T(8,128)(2,1)S(1)}, bf16[192,256]{1,0:T(8,128)(2,1)S(1)}, u32[]{:S(2)}, u32[]{:S(2)}) collective-permute-start(bf16[192,256]{1,0:T(8,128)(2,1)S(1)} %collective-permute-done.3), channel_id=1, source_target_pairs={{0,2},{2,4},{4,6},{6,8},{8,10},{10,12},{12,14},{14,16},{16,18},{18... | collective-permute-start | bytes 294920 | tf_op jit(solution)/shard_map/ppermute | solution.py:20
  49.1 6.7 %collective-permute-start.5 = (bf16[192,256]{1,0:T(8,128)(2,1)S(1)}, bf16[192,256]{1,0:T(8,128)(2,1)S(1)}, u32[]{:S(2)}, u32[]{:S(2)}) collective-permute-start(bf16[192,256]{1,0:T(8,128)(2,1)S(1)} %collective-permute-done.4), channel_id=1, source_target_pairs={{0,2},{2,4},{4,6},{6,8},{8,10},{10,12},{12,14},{14,16},{16,18},{18... | collective-permute-start | bytes 294920 | tf_op jit(solution)/shard_map/ppermute | solution.py:20
  55.8 6.7 %collective-permute-start.6 = (bf16[192,256]{1,0:T(8,128)(2,1)S(1)}, bf16[192,256]{1,0:T(8,128)(2,1)S(1)}, u32[]{:S(2)}, u32[]{:S(2)}) collective-permute-start(bf16[192,256]{1,0:T(8,128)(2,1)S(1)} %collective-permute-done.5), channel_id=1, source_target_pairs={{0,2},{2,4},{4,6},{6,8},{8,10},{10,12},{12,14},{14,16},{16,18},{18... | collective-permute-start | bytes 294920 | tf_op jit(solution)/shard_map/ppermute | solution.py:20
  62.6 6.7 %collective-permute-start.7 = (bf16[192,256]{1,0:T(8,128)(2,1)S(1)}, bf16[192,256]{1,0:T(8,128)(2,1)S(1)}, u32[]{:S(2)}, u32[]{:S(2)}) collective-permute-start(bf16[192,256]{1,0:T(8,128)(2,1)S(1)} %collective-permute-done.6), channel_id=1, source_target_pairs={{0,2},{2,4},{4,6},{6,8},{8,10},{10,12},{12,14},{14,16},{16,18},{18... | collective-permute-start | bytes 294920 | tf_op jit(solution)/shard_map/ppermute | solution.py:20
  69.3 6.7 %collective-permute-start.8 = (bf16[192,256]{1,0:T(8,128)(2,1)S(1)}, bf16[192,256]{1,0:T(8,128)(2,1)S(1)}, u32[]{:S(2)}, u32[]{:S(2)}) collective-permute-start(bf16[192,256]{1,0:T(8,128)(2,1)S(1)} %collective-permute-done.7), channel_id=1, source_target_pairs={{0,2},{2,4},{4,6},{6,8},{8,10},{10,12},{12,14},{14,16},{16,18},{18... | collective-permute-start | bytes 294920 | tf_op jit(solution)/shard_map/ppermute | solution.py:20
  76.1 6.7 %collective-permute-start.9 = (bf16[192,256]{1,0:T(8,128)(2,1)S(1)}, bf16[192,256]{1,0:T(8,128)(2,1)S(1)}, u32[]{:S(2)}, u32[]{:S(2)}) collective-permute-start(bf16[192,256]{1,0:T(8,128)(2,1)S(1)} %collective-permute-done.8), channel_id=1, source_target_pairs={{0,2},{2,4},{4,6},{6,8},{8,10},{10,12},{12,14},{14,16},{16,18},{18... | collective-permute-start | bytes 294920 | tf_op jit(solution)/shard_map/ppermute | solution.py:20
  82.8 6.7 %collective-permute-start.10 = (bf16[192,256]{1,0:T(8,128)(2,1)S(1)}, bf16[192,256]{1,0:T(8,128)(2,1)S(1)}, u32[]{:S(2)}, u32[]{:S(2)}) collective-permute-start(bf16[192,256]{1,0:T(8,128)(2,1)S(1)} %collective-permute-done.9), channel_id=1, source_target_pairs={{0,2},{2,4},{4,6},{6,8},{8,10},{10,12},{12,14},{14,16},{16,18},{18... | collective-permute-start | bytes 294920 | tf_op jit(solution)/shard_map/ppermute | solution.py:20
  89.5 6.7 %collective-permute-start.11 = (bf16[192,256]{1,0:T(8,128)(2,1)S(1)}, bf16[192,256]{1,0:T(8,128)(2,1)S(1)}, u32[]{:S(2)}, u32[]{:S(2)}) collective-permute-start(bf16[192,256]{1,0:T(8,128)(2,1)S(1)} %collective-permute-done.10), channel_id=1, source_target_pairs={{0,2},{2,4},{4,6},{6,8},{8,10},{10,12},{12,14},{14,16},{16,18},{18... | collective-permute-start | bytes 294920 | tf_op jit(solution)/shard_map/ppermute | solution.py:20
  96.3 6.7 %collective-permute-start.12 = (bf16[192,256]{1,0:T(8,128)(2,1)S(1)}, bf16[192,256]{1,0:T(8,128)(2,1)S(1)}, u32[]{:S(2)}, u32[]{:S(2)}) collective-permute-start(bf16[192,256]{1,0:T(8,128)(2,1)S(1)} %collective-permute-done.11), channel_id=1, source_target_pairs={{0,2},{2,4},{4,6},{6,8},{8,10},{10,12},{12,14},{14,16},{16,18},{18... | collective-permute-start | bytes 294920 | tf_op jit(solution)/shard_map/ppermute | solution.py:20
  103.0 6.7 %collective-permute-start.13 = (bf16[192,256]{1,0:T(8,128)(2,1)S(1)}, bf16[192,256]{1,0:T(8,128)(2,1)S(1)}, u32[]{:S(2)}, u32[]{:S(2)}) collective-permute-start(bf16[192,256]{1,0:T(8,128)(2,1)S(1)} %collective-permute-done.12), channel_id=1, source_target_pairs={{0,2},{2,4},{4,6},{6,8},{8,10},{10,12},{12,14},{14,16},{16,18},{18... | collective-permute-start | bytes 294920 | tf_op jit(solution)/shard_map/ppermute | solution.py:20
  109.8 6.7 %collective-permute-start.14 = (bf16[192,256]{1,0:T(8,128)(2,1)S(1)}, bf16[192,256]{1,0:T(8,128)(2,1)S(1)}, u32[]{:S(2)}, u32[]{:S(2)}) collective-permute-start(bf16[192,256]{1,0:T(8,128)(2,1)S(1)} %collective-permute-done.13), channel_id=1, source_target_pairs={{0,2},{2,4},{4,6},{6,8},{8,10},{10,12},{12,14},{14,16},{16,18},{18... | collective-permute-start | bytes 294920 | tf_op jit(solution)/shard_map/ppermute | solution.py:20
  136.2 1.0 copy-start
  139.1 0.8 copy-start.1
  141.5 1.0 copy-start
  144.4 0.8 copy-start.1
  146.9 1.0 copy-start
  149.7 0.8 copy-start.1
  152.2 1.2 copy-start
  155.3 0.8 copy-start.1
  157.8 1.0 copy-start
  160.6 0.8 copy-start.1
  163.1 1.0 copy-start
  166.0 0.8 copy-start.1
  168.2 10.9 %copy-start.4 = (f32[2048]{0:T(1024)S(1)}, f32[2048]{0:T(1024)}, u32[]{:S(2)}) copy-start(f32[2048]{0:T(1024)} %param.20) | copy-start | bytes 24580
Sparse Core Ops, SparseCore 0:
  9.6 43.5 all-gather.5
  54.8 55.5 all-gather.7
  112.7 93.9 all-gather.9
  208.8 92.2 all-gather.11
  303.1 95.1 all-gather.13
  412.2 15.6 reduce-scatter.1
